TPU v7x, 32 devices: a whole 2x2x4 slice. The times are simulated.
32 devices in a mesh: ra: 8 (over z, y), cb: 4 (over x, core).
Axes of the slice: x: 2, y: 2, z: 4, core: 2. Of those that a mesh axis runs over, the one named last changes fastest.
Arguments:
- stream: bfloat16 [64, 1024], P(None, 'ra'), may hold values from -24 to 24, as said below
- gain_first: float32 [1024], P('ra'), may hold values from 0.5 to 1.5
- up_first: float32 [1024, 4096], P('ra', 'cb'), may hold values from -0.1875 to 0.1875
- down_first: float32 [4096, 1024], P('cb', 'ra'), may hold values from -0.09375 to 0.09375
- gain_second: float32 [1024], P('ra'), may hold values from 0.5 to 1.5
- up_second: float32 [1024, 4096], P('ra', 'cb'), may hold values from -0.1875 to 0.1875
- down_second: float32 [4096, 1024], P('cb', 'ra'), may hold values from -0.09375 to 0.09375
Outputs:
- read: bfloat16 [64, 1024], P(None, 'ra')
Inputs may be any that keep to these rules, and one draw needn't show every extreme that they name: stream is of order one, and in each token one aligned block of 128 features is four times larger than the rest.
All inputs are finite; a program needn't handle non-finite values.
Results may differ from a plain program's by a relative error of at most 0.025.
Values may be sent and summed in bfloat16 or wider, within the bound.
A program may use at most 64 MiB of HBM per device.

v0:
```python
import jax
import jax.numpy as jnp
from jax import lax
from jax.sharding import PartitionSpec as P

D = 1024
EPS = 1e-06
RESIDUAL = 0.25


def sublayer(stream, norm_gain, w_up, w_down):
    floated = stream.astype(jnp.float32)
    own_squares = jnp.sum(floated * floated, axis=1, keepdims=True)
    squares = lax.psum(own_squares, "ra")
    factor = lax.rsqrt(squares / D + EPS)
    normed = (floated * factor * norm_gain.astype(jnp.float32)[None, :]).astype(jnp.bfloat16)
    up_bf = w_up.astype(jnp.bfloat16)
    down_bf = w_down.astype(jnp.bfloat16)
    partial_value = jnp.dot(normed, up_bf, preferred_element_type=jnp.float32)
    preact = lax.psum(partial_value, "ra")
    activated = jnp.square(jax.nn.relu(preact)).astype(jnp.bfloat16)
    down_part = jnp.dot(activated, down_bf, preferred_element_type=jnp.float32)
    branch = lax.psum(down_part.astype(jnp.bfloat16), "cb").astype(jnp.float32)
    return (RESIDUAL * floated + branch).astype(jnp.bfloat16)


def local(stream, gain_first, up_first, down_first, gain_second, up_second, down_second):
    middle = sublayer(stream, gain_first, up_first, down_first)
    return sublayer(middle, gain_second, up_second, down_second)


def solution(mesh):
    return jax.shard_map(
        local,
        mesh=mesh,
        in_specs=(
            P(None, "ra"),
            P("ra"),
            P("ra", "cb"),
            P("cb", "ra"),
            P("ra"),
            P("ra", "cb"),
            P("cb", "ra"),
        ),
        out_specs=P(None, "ra"),
        check_vma=False,
    )
```

profile of v0, /device:TPU:0, one launch (start us, length us, event | category | flops | bytes accessed | tf_op | source)
XLA Modules:
  0.0 221.5 jit_solution(7013383935762173612)
XLA Ops:
  6.5 0.0 copy-start.3
  6.5 0.0 all-reduce.3.cloned.1.call-start
  6.5 0.9 fusion.10
  7.4 23.2 %psum.42 = f32[64,1]{0,1:T(1,128)S(1)} all-reduce(f32[64,1]{0,1:T(1,128)S(1)} %bitcast.7), channel_id=1, replica_groups=mesh['ra'=8,'cb'=4] {'ra'}, use_global_device_ids=true, to_apply=%region_1.0 | all-reduce | flops 64 | bytes 512 | tf_op jit(solution)/shard_map/psum | solution.py:14
  30.6 0.0 copy-done.3
  30.6 0.6 copy-done.4
  31.2 2.0 fusion.4
  33.3 0.0 all-reduce.3.cloned.1.call-update
  33.3 0.0 all-reduce.5.cloned.1.call-start
  33.4 68.4 %all-reduce.3.cloned.1.call-done = f32[64,1024]{1,0:T(8,128)} async-done(((f32[64,1024]{1,0:T(8,128)}), f32[64,1024]{1,0:T(8,128)}) %all-reduce.3.cloned.1.call-update) | async-done | bytes 262160 | tf_op jit(solution)/shard_map/psum | solution.py:20
  101.7 0.0 copy-done.1
  101.7 1.1 convolution_convert_fusion.1
  102.8 10.1 %psum.44 = bf16[64,128]{1,0:T(8,128)(2,1)S(1)} all-reduce(bf16[64,128]{1,0:T(8,128)(2,1)S(1)} %convolution_convert_fusion.1), channel_id=1, replica_groups=mesh['ra'=8,'cb'=4] {'cb'}, use_global_device_ids=true, to_apply=%region_3.4 | all-reduce | flops 8192 | bytes 32768 | tf_op jit(solution)/shard_map/psum | solution.py:23
  113.0 0.1 fusion.15
  113.1 19.6 %psum.45 = f32[64,1]{0,1:T(1,128)S(1)} all-reduce(f32[64,1]{0,1:T(1,128)S(1)} %bitcast.6), channel_id=1, replica_groups=mesh['ra'=8,'cb'=4] {'ra'}, use_global_device_ids=true, to_apply=%region_5.6 | all-reduce | flops 64 | bytes 512 | tf_op jit(solution)/shard_map/psum | solution.py:14
  132.7 0.0 copy-done
  132.7 0.6 copy-done.5
  133.3 0.9 fusion.1
  134.3 0.0 all-reduce.5.cloned.1.call-update
  134.3 68.5 %all-reduce.5.cloned.1.call-done = f32[64,1024]{1,0:T(8,128)} async-done(((f32[64,1024]{1,0:T(8,128)}), f32[64,1024]{1,0:T(8,128)}) %all-reduce.5.cloned.1.call-update) | async-done | bytes 262160 | tf_op jit(solution)/shard_map/psum | solution.py:20
  202.8 0.0 copy-done.2
  202.8 1.1 convolution_convert_fusion
  203.9 10.1 %psum.47 = bf16[64,128]{1,0:T(8,128)(2,1)S(1)} all-reduce(bf16[64,128]{1,0:T(8,128)(2,1)S(1)} %convolution_convert_fusion), channel_id=1, replica_groups=mesh['ra'=8,'cb'=4] {'cb'}, use_global_device_ids=true, to_apply=%region_7.8 | all-reduce | flops 8192 | bytes 32768 | tf_op jit(solution)/shard_map/psum | solution.py:23
  214.1 0.6 fusion.14
  (7 shorter events, 0.0 us)
Async XLA Ops:
  6.5 24.1 %copy-start.3 = (bf16[64,128]{1,0:T(8,128)(2,1)S(1)}, bf16[64,128]{1,0:T(8,128)(2,1)}, u32[]{:S(2)}) copy-start(bf16[64,128]{1,0:T(8,128)(2,1)} %param.7) | copy-start | bytes 49156
  6.5 95.2 %all-reduce.3.cloned.1.call-start = ((), (), s32[]{:S(2)}) async-start(), calls=%async_computation | async-start | bytes 524288 | tf_op jit(solution)/shard_map/psum | solution.py:20
  30.6 0.7 copy-start.4
  31.2 70.5 %copy-start.1 = (f32[1024,128]{1,0:T(8,128)S(1)}, f32[1024,128]{1,0:T(8,128)}, u32[]{:S(2)}) copy-start(f32[1024,128]{1,0:T(8,128)} %param.10) | copy-start | bytes 1572868
  33.3 99.4 %copy-start = (f32[128,1024]{1,0:T(8,128)S(1)}, f32[128,1024]{1,0:T(8,128)}, u32[]{:S(2)}) copy-start(f32[128,1024]{1,0:T(8,128)} %param.12) | copy-start | bytes 1572868
  33.3 169.5 %all-reduce.5.cloned.1.call-start = ((), (), s32[]{:S(2)}) async-start(), calls=%async_computation.1 | async-start | bytes 524288 | tf_op jit(solution)/shard_map/psum | solution.py:20
  132.7 0.7 copy-start.5
  133.3 69.5 %copy-start.2 = (f32[1024,128]{1,0:T(8,128)S(1)}, f32[1024,128]{1,0:T(8,128)}, u32[]{:S(2)}) copy-start(f32[1024,128]{1,0:T(8,128)} %param.13) | copy-start | bytes 1572868
Sparse Core Ops, SparseCore 0:
  33.4 68.2 all-reduce.2
  134.4 68.3 all-reduce.4
where the time goes:
time: 222 us
  waiting for transfers between devices  137 us (62%)
  blocking collectives  63 us (28%)
  between operations  13.4 us (6%)
  matrix products  5.2 us (2%)
    psum x2, waiting for transfers between devices, sublayer(): preact = lax.psum(partial_value, 'ra')  137 us
    psum x2, blocking collectives, sublayer(): squares = lax.psum(own_squares, 'ra')  42.8 us
    psum x2, blocking collectives, sublayer(): branch = lax.psum(down_part.astype(jnp.bfloat16), 'cb').astype(jnp.float32)  20.2 us
  transfers between devices with their start and end apart: 2, of which 2 were waited for; matrix products, arithmetic and copies ran while one was open for 0% of the time, Pallas kernels for 0%

commit v1 on v0

--- a/solution.py
+++ b/solution.py
@@ -11,7 +11,9 @@
 def sublayer(stream, norm_gain, w_up, w_down):
     floated = stream.astype(jnp.float32)
     own_squares = jnp.sum(floated * floated, axis=1, keepdims=True)
-    squares = lax.psum(own_squares, "ra")
+    squares = own_squares
+    for hop in (1, 2, 4):
+        squares = squares + lax.ppermute(squares, "ra", [(dev, dev ^ hop) for dev in range(8)])
     factor = lax.rsqrt(squares / D + EPS)
     normed = (floated * factor * norm_gain.astype(jnp.float32)[None, :]).astype(jnp.bfloat16)
     up_bf = w_up.astype(jnp.bfloat16)

time: 222 us -> 209 us (0.941)
  blocking collectives: 63 us -> 20.2 us
  waiting for transfers between devices: 137 us -> 156 us
  starting transfers between devices: 0.04 us -> 11.6 us
    psum x2 -> x0, blocking collectives: 42.8 us -> none  [sublayer(): squares = lax.psum(own_squares, 'ra')]
    ppermute x0 -> x6, waiting for transfers between devices: none -> 12.9 us  [sublayer(): lax.ppermute(squares, 'ra', [(dev, dev ^ hop) for dev in range(8)])]
    ppermute x0 -> x6, starting transfers between devices: none -> 11.5 us  [sublayer(): lax.ppermute(squares, 'ra', [(dev, dev ^ hop) for dev in range(8)])]
    psum x2, waiting for transfers between devices: 137 us -> 143 us  [sublayer(): preact = lax.psum(partial_value, 'ra')]
  transfers between devices with their start and end apart: 2 -> 8, of which waited for: 2 -> 8; matrix products, arithmetic and copies ran while one was open for 0% -> 0% of each run, Pallas kernels for 0% -> 0%
where the time goes in v1:
time: 209 us; the launch traced here: 208 us
  waiting for transfers between devices  156 us (75%)
  blocking collectives  20.2 us (10%)
  between operations  13.5 us (6%)
  starting transfers between devices  11.6 us (6%)
  matrix products  5.2 us (2%)
    psum x2, waiting for transfers between devices, sublayer(): preact = lax.psum(partial_value, 'ra')  143 us
    psum x2, blocking collectives, sublayer(): branch = lax.psum(down_part.astype(jnp.bfloat16), 'cb').astype(jnp.float32)  20.2 us
    ppermute x6, waiting for transfers between devices, sublayer(): lax.ppermute(squares, 'ra', [(dev, dev ^ hop) for dev in range(8)])  12.9 us
    ppermute x6, starting transfers between devices, sublayer(): lax.ppermute(squares, 'ra', [(dev, dev ^ hop) for dev in range(8)])  11.5 us
  transfers between devices with their start and end apart: 8, of which 8 were waited for; matrix products, arithmetic and copies ran while one was open for 0% of the time, Pallas kernels for 0%

profile of v1, /device:TPU:0, one launch (start us, length us, event | category | flops | bytes accessed | tf_op | source)
XLA Modules:
  0.0 208.3 jit_solution(8864792584479702560)
XLA Ops:
  6.5 0.9 fusion.10
  7.4 3.1 %collective-permute-start = (f32[64,1]{0,1:T(1,128)S(1)}, f32[64,1]{0,1:T(1,128)S(1)}, u32[]{:S(2)}, u32[]{:S(2)}) collective-permute-start(f32[64,1]{0,1:T(1,128)S(1)} %bitcast.9), channel_id=1, source_target_pairs={{0,4},{4,0},{8,12},{12,8},{16,20},{20,16},{24,28},{28,24},{1,5},{5... | collective-permute-start | bytes 776 | tf_op jit(solution)/shard_map/ppermute | solution.py:16
  10.5 1.5 collective-permute-done
  12.0 2.1 collective-permute-start.1
  14.1 1.5 collective-permute-done.1
  15.7 3.0 %collective-permute-start.2 = (f32[64,1]{0,1:T(1,128)S(1)}, f32[64,1]{0,1:T(1,128)S(1)}, u32[]{:S(2)}, u32[]{:S(2)}) collective-permute-start(f32[64,1]{0,1:T(1,128)S(1)} %add.39), channel_id=1, source_target_pairs={{0,16},{4,20},{8,24},{12,28},{16,0},{20,4},{24,8},{28,12},{1,17},{... | collective-permute-start | bytes 776 | tf_op jit(solution)/shard_map/ppermute | solution.py:16
  18.7 1.5 collective-permute-done.2
  20.3 2.0 fusion.4
  22.3 0.0 all-reduce.5.cloned.1.call-start
  22.4 72.7 %all-reduce.3.cloned.1.call-done = f32[64,1024]{1,0:T(8,128)} async-done(((f32[64,1024]{1,0:T(8,128)}), f32[64,1024]{1,0:T(8,128)}) %all-reduce.3.cloned.1.call-update) | async-done | bytes 262160 | tf_op jit(solution)/shard_map/psum | solution.py:22
  95.1 1.1 convolution_convert_fusion.1
  96.2 10.1 %psum.29 = bf16[64,128]{1,0:T(8,128)(2,1)S(1)} all-reduce(bf16[64,128]{1,0:T(8,128)(2,1)S(1)} %convolution_convert_fusion.1), channel_id=1, replica_groups=mesh['ra'=8,'cb'=4] {'cb'}, use_global_device_ids=true, to_apply=%region_2.3 | all-reduce | flops 8192 | bytes 32768 | tf_op jit(solution)/shard_map/psum | solution.py:25
  106.3 0.1 fusion.15
  106.4 0.7 collective-permute-start.3
  107.2 2.9 %collective-permute-done.3 = f32[64,1]{0,1:T(1,128)S(1)} collective-permute-done((f32[64,1]{0,1:T(1,128)S(1)}, f32[64,1]{0,1:T(1,128)S(1)}, u32[]{:S(2)}, u32[]{:S(2)}) %collective-permute-start.3) | collective-permute-done | bytes 288 | tf_op jit(solution)/shard_map/ppermute | solution.py:16
  110.1 1.0 collective-permute-start.4
  111.1 2.6 %collective-permute-done.4 = f32[64,1]{0,1:T(1,128)S(1)} collective-permute-done((f32[64,1]{0,1:T(1,128)S(1)}, f32[64,1]{0,1:T(1,128)S(1)}, u32[]{:S(2)}, u32[]{:S(2)}) %collective-permute-start.4) | collective-permute-done | bytes 288 | tf_op jit(solution)/shard_map/ppermute | solution.py:16
  113.6 1.7 collective-permute-start.5
  115.3 2.8 %collective-permute-done.5 = f32[64,1]{0,1:T(1,128)S(1)} collective-permute-done((f32[64,1]{0,1:T(1,128)S(1)}, f32[64,1]{0,1:T(1,128)S(1)}, u32[]{:S(2)}, u32[]{:S(2)}) %collective-permute-start.5) | collective-permute-done | bytes 288 | tf_op jit(solution)/shard_map/ppermute | solution.py:16
  118.1 0.9 fusion.1
  119.1 70.5 %all-reduce.5.cloned.1.call-done = f32[64,1024]{1,0:T(8,128)} async-done(((f32[64,1024]{1,0:T(8,128)}), f32[64,1024]{1,0:T(8,128)}) %all-reduce.5.cloned.1.call-update) | async-done | bytes 262160 | tf_op jit(solution)/shard_map/psum | solution.py:22
  189.6 1.1 convolution_convert_fusion
  190.7 10.1 %psum.31 = bf16[64,128]{1,0:T(8,128)(2,1)S(1)} all-reduce(bf16[64,128]{1,0:T(8,128)(2,1)S(1)} %convolution_convert_fusion), channel_id=1, replica_groups=mesh['ra'=8,'cb'=4] {'cb'}, use_global_device_ids=true, to_apply=%region_5.6 | all-reduce | flops 8192 | bytes 32768 | tf_op jit(solution)/shard_map/psum | solution.py:25
  200.8 0.6 fusion.14
  (21 shorter events, 0.1 us)
Async XLA Ops:
  6.5 13.7 %copy-start.3 = (bf16[64,128]{1,0:T(8,128)(2,1)S(1)}, bf16[64,128]{1,0:T(8,128)(2,1)}, u32[]{:S(2)}) copy-start(bf16[64,128]{1,0:T(8,128)(2,1)} %param.7) | copy-start | bytes 49156
  6.5 88.5 %all-reduce.3.cloned.1.call-start = ((), (), s32[]{:S(2)}) async-start(), calls=%async_computation | async-start | bytes 524288 | tf_op jit(solution)/shard_map/psum | solution.py:22
  7.4 4.6 %collective-permute-start = (f32[64,1]{0,1:T(1,128)S(1)}, f32[64,1]{0,1:T(1,128)S(1)}, u32[]{:S(2)}, u32[]{:S(2)}) collective-permute-start(f32[64,1]{0,1:T(1,128)S(1)} %bitcast.9), channel_id=1, source_target_pairs={{0,4},{4,0},{8,12},{12,8},{16,20},{20,16},{24,28},{28,24},{1,5},{5... | collective-permute-start | bytes 776 | tf_op jit(solution)/shard_map/ppermute | solution.py:16
  12.0 3.6 %collective-permute-start.1 = (f32[64,1]{0,1:T(1,128)S(1)}, f32[64,1]{0,1:T(1,128)S(1)}, u32[]{:S(2)}, u32[]{:S(2)}) collective-permute-start(f32[64,1]{0,1:T(1,128)S(1)} %bitcast_add_fusion.1), channel_id=1, source_target_pairs={{0,8},{4,12},{8,0},{12,4},{16,24},{20,28},{24,16},{28,20},{1,9},{5... | collective-permute-start | bytes 776 | tf_op jit(solution)/shard_map/ppermute | solution.py:16
  15.7 4.6 %copy-start.4 = (f32[128]{0:T(128)S(1)}, f32[128]{0:T(128)}, u32[]{:S(2)}) copy-start(f32[128]{0:T(128)} %param.8) | copy-start | bytes 1540
  15.7 4.6 %collective-permute-start.2 = (f32[64,1]{0,1:T(1,128)S(1)}, f32[64,1]{0,1:T(1,128)S(1)}, u32[]{:S(2)}, u32[]{:S(2)}) collective-permute-start(f32[64,1]{0,1:T(1,128)S(1)} %add.39), channel_id=1, source_target_pairs={{0,16},{4,20},{8,24},{12,28},{16,0},{20,4},{24,8},{28,12},{1,17},{... | collective-permute-start | bytes 776 | tf_op jit(solution)/shard_map/ppermute | solution.py:16
  20.3 74.8 %copy-start.1 = (f32[1024,128]{1,0:T(8,128)S(1)}, f32[1024,128]{1,0:T(8,128)}, u32[]{:S(2)}) copy-start(f32[1024,128]{1,0:T(8,128)} %param.10) | copy-start | bytes 1572868
  22.3 95.8 %copy-start = (f32[128,1024]{1,0:T(8,128)S(1)}, f32[128,1024]{1,0:T(8,128)}, u32[]{:S(2)}) copy-start(f32[128,1024]{1,0:T(8,128)} %param.12) | copy-start | bytes 1572868
  22.3 167.2 %all-reduce.5.cloned.1.call-start = ((), (), s32[]{:S(2)}) async-start(), calls=%async_computation.1 | async-start | bytes 524288 | tf_op jit(solution)/shard_map/psum | solution.py:22
  106.4 3.6 %collective-permute-start.3 = (f32[64,1]{0,1:T(1,128)S(1)}, f32[64,1]{0,1:T(1,128)S(1)}, u32[]{:S(2)}, u32[]{:S(2)}) collective-permute-start(f32[64,1]{0,1:T(1,128)S(1)} %bitcast.8), channel_id=1, source_target_pairs={{0,4},{4,0},{8,12},{12,8},{16,20},{20,16},{24,28},{28,24},{1,5},{5... | collective-permute-start | bytes 776 | tf_op jit(solution)/shard_map/ppermute | solution.py:16
  110.1 3.6 %collective-permute-start.4 = (f32[64,1]{0,1:T(1,128)S(1)}, f32[64,1]{0,1:T(1,128)S(1)}, u32[]{:S(2)}, u32[]{:S(2)}) collective-permute-start(f32[64,1]{0,1:T(1,128)S(1)} %bitcast_add_fusion), channel_id=1, source_target_pairs={{0,8},{4,12},{8,0},{12,4},{16,24},{20,28},{24,16},{28,20},{1,9},{5... | collective-permute-start | bytes 776 | tf_op jit(solution)/shard_map/ppermute | solution.py:16
  113.6 4.5 %copy-start.5 = (f32[128]{0:T(128)S(1)}, f32[128]{0:T(128)}, u32[]{:S(2)}) copy-start(f32[128]{0:T(128)} %param.11) | copy-start | bytes 1540
  113.6 4.5 %collective-permute-start.5 = (f32[64,1]{0,1:T(1,128)S(1)}, f32[64,1]{0,1:T(1,128)S(1)}, u32[]{:S(2)}, u32[]{:S(2)}) collective-permute-start(f32[64,1]{0,1:T(1,128)S(1)} %add.44), channel_id=1, source_target_pairs={{0,16},{4,20},{8,24},{12,28},{16,0},{20,4},{24,8},{28,12},{1,17},{... | collective-permute-start | bytes 776 | tf_op jit(solution)/shard_map/ppermute | solution.py:16
  118.1 71.5 %copy-start.2 = (f32[1024,128]{1,0:T(8,128)S(1)}, f32[1024,128]{1,0:T(8,128)}, u32[]{:S(2)}) copy-start(f32[1024,128]{1,0:T(8,128)} %param.13) | copy-start | bytes 1572868
Sparse Core Ops, SparseCore 0:
  22.5 72.5 all-reduce.2
  119.2 70.3 all-reduce.4
